TPU v7x, 32 devices: a whole 2x2x4 slice. The times are simulated.
32 devices in a mesh: sp: 8 (over z, x), tp: 4 (over y, core).
Axes of the slice: x: 2, y: 2, z: 4, core: 2. Of those that a mesh axis runs over, the one named last changes fastest.
Arguments:
- tokens: bfloat16 [1024, 2048], P('sp', 'tp'), may hold values from -6 to 6
- norm_gain: float32 [2048], replicated, may hold values from 0.1 to 1.9
- da_query: bfloat16 [2048, 1024], P(None, 'tp'), as said below
- da_key: bfloat16 [2048, 1024], P(None, 'tp'), may hold values from -0.125 to 0.125
- da_value: bfloat16 [2048, 1024], P(None, 'tp'), may hold values from -0.125 to 0.125
- mix_lambda: float32 [8], P('tp'), may hold values from 0.3 to 0.8
- attn_gain: float32 [128], replicated, may hold values from 0.1 to 1.9
- rec_query: bfloat16 [2048, 1024], P(None, 'tp'), may hold values from -0.125 to 0.125
- rec_forget_fwd: bfloat16 [2048, 1024], P(None, 'tp'), may hold values from -0.375 to 0.375
- rec_forget_bwd: bfloat16 [2048, 1024], P(None, 'tp'), may hold values from -0.375 to 0.375
- rec_value: bfloat16 [2048, 1024], P(None, 'tp'), may hold values from -0.125 to 0.125
- gate_gap: float32 [2, 1024], P(None, 'tp'), may hold values from 0.0009765625 to 0.12
- extra_decay: float32 [2, 1024, 8], P(None, 'sp', 'tp'), may hold values from -0.7 to 0
- init_state: float32 [2, 8, 128, 128], P(None, 'tp'), may hold values from -1.5 to 1.5
- rec_gain: float32 [128], replicated, may hold values from 0.1 to 1.9
- out_attn: bfloat16 [1024, 2048], P('tp'), may hold values from -0.125 to 0.125
- out_rec: bfloat16 [1024, 2048], P('tp'), may hold values from -0.125 to 0.125
Outputs:
- mixed: bfloat16 [1024, 2048], P(('sp', 'tp'))
Inputs may be any that keep to these rules, and one draw needn't show every extreme that they name: `da_query`: entries lie within -240 / sqrt(2048) and 240 / sqrt(2048).
All inputs are finite; a program needn't handle non-finite values.
Results may differ from a plain program's by a relative error of at most 0.014.
The roundings to bfloat16 on the way count: a program that leaves them out, or rounds other values in their place, can miss the bound.
Values may be sent and summed in bfloat16 or wider, within the bound.
A program may use at most 128 MiB of HBM per device.

v0:
```python
import jax
import jax.numpy as jnp
from jax import lax
from jax.sharding import PartitionSpec as P

D = 2048
QK_DIM = 64
DA_VAL = 128
HG_KEY = 128
HG_VAL = 128
SPAN = 64
EPSILON = 1e-06
EXACT_PRECISION = lax.Precision.HIGHEST


def prefix(value, axis, join, neutral, backward):
    count = lax.axis_size(axis)
    place = lax.axis_index(axis)
    ahead = count - 1 - place if backward else place
    gathered = jax.tree.map(
        lambda a, kind: lax.all_gather(a.astype(kind), axis), value, (jnp.bfloat16, jnp.bfloat16)
    )
    state = jax.tree.map(lambda a, e: jnp.zeros_like(a) + jnp.asarray(e, a.dtype), value, neutral)

    def one(lap, state):
        source = count - 1 - lap if backward else lap
        return join(
            state,
            jax.tree.map(
                lambda a, own: lax.dynamic_index_in_dim(a, source, 0, False).astype(own.dtype),
                gathered,
                value,
            ),
        )

    return lax.fori_loop(0, ahead, one, state)


def block_scan(query, key_in, values, log_decay, initial):
    length = query.shape[0]
    count = length // SPAN

    def split(array):
        return array.reshape((count, SPAN) + array.shape[1:])

    lower = jnp.tril(jnp.ones((SPAN, SPAN), jnp.float32))

    def block_one_step(carried_state, inputs):
        query_tile, key_tile, value_tile, g_block = inputs
        cumulative_decay = jnp.cumsum(g_block, axis=0)
        relative = cumulative_decay[:, None] - cumulative_decay[None, :]
        relative = jnp.where(lower[:, :, None, None] > 0, relative, -jnp.inf)
        score_matrix = jnp.einsum(
            "ihk,ijhk,jhk->hij", query_tile, jnp.exp(relative), key_tile, precision=EXACT_PRECISION
        )
        output_rows = jnp.einsum(
            "ujg,jga->uja",
            query_tile * jnp.exp(cumulative_decay),
            carried_state,
            precision=EXACT_PRECISION,
        ) + jnp.einsum("ots,sok->tok", score_matrix, value_tile, precision=EXACT_PRECISION)
        ending_state = cumulative_decay[-1]
        carried_state = jnp.exp(ending_state)[..., None] * carried_state + jnp.einsum(
            "zds,zdx->dsx",
            key_tile * jnp.exp(ending_state[None] - cumulative_decay),
            value_tile,
            precision=EXACT_PRECISION,
        )
        return (carried_state, output_rows)

    carried_state, output_rows = lax.scan(
        block_one_step, initial, (split(query), split(key_in), split(values), split(log_decay))
    )
    return (output_rows.reshape((length,) + output_rows.shape[2:]), carried_state)


def combine_states(earlier, later):
    return (earlier[0] + later[0], jnp.exp(later[0])[..., None] * earlier[1] + later[1])


def local(
    tokens,
    norm_gain,
    da_query,
    da_key,
    da_value,
    mix_lambda,
    attn_gain,
    rec_query,
    rec_forget_fwd,
    rec_forget_bwd,
    rec_value,
    gate_gap,
    extra_decay,
    init_state,
    rec_gain,
    out_attn,
    out_rec,
):
    row_count = tokens.shape[0]
    weight_list = (da_query, da_key, da_value, rec_query, rec_forget_fwd, rec_forget_bwd, rec_value)
    values = lax.all_gather(tokens, "tp", axis=1, tiled=True).astype(jnp.float32)
    scaled = (values * norm_gain).astype(jnp.bfloat16)
    updated = tuple(
        (jnp.dot(scaled, weight, preferred_element_type=jnp.float32) for weight in weight_list)
    )
    squares = jnp.sum(values * values, axis=1)
    inv_rms = lax.rsqrt(squares / D + EPSILON)[:, None]
    query_att, key_att, value_att, query_rec, forget_fwd, forget_bwd, value_rec = tuple(
        ((total_now * inv_rms).astype(jnp.bfloat16) for total_now in updated)
    )
    head_count = mix_lambda.shape[0]
    queries = query_att.reshape(row_count, head_count, 2, QK_DIM)
    rec_heads = query_rec.shape[1] // HG_KEY

    def heads(array, width):
        return array.astype(jnp.float32).reshape(row_count, rec_heads, width)

    start_state = (
        jnp.full((head_count, 2, row_count), -jnp.inf, jnp.float32),
        jnp.zeros((head_count, 2, row_count), jnp.float32),
        jnp.zeros((head_count, 2, row_count, DA_VAL), jnp.float32),
    )
    running = start_state
    key_piece = lax.all_gather(key_att, "sp", axis=0, tiled=True)
    value_piece = lax.all_gather(value_att, "sp", axis=0, tiled=True)
    length = key_piece.shape[0]
    step_rows = max((candidate for candidate in range(1, 2049) if length % candidate == 0))
    key_blocks = key_piece.reshape(length // step_rows, step_rows, head_count, 2, QK_DIM)
    value_blocks = value_piece.reshape(length // step_rows, step_rows, head_count, DA_VAL)

    def absorb_one_step(carried_state, inputs):
        maxima, denoms, numerator = carried_state
        key_block, value_block = inputs
        score_matrix = jnp.einsum(
            "qhmd,khmd->hmqk", queries, key_block, preferred_element_type=jnp.float32
        ) * QK_DIM ** (-0.5)
        new_maxima = jnp.maximum(maxima, jnp.max(score_matrix, axis=3))
        factor = jnp.exp(maxima - new_maxima)
        unnorm = jnp.exp(score_matrix - new_maxima[..., None])
        denoms = denoms * factor + jnp.sum(unnorm, axis=3)
        numerator = numerator * factor[..., None] + jnp.einsum(
            "hmqk,khv->hmqv",
            unnorm.astype(jnp.bfloat16),
            value_block,
            preferred_element_type=jnp.float32,
        )
        return ((new_maxima, denoms, numerator), None)

    running, unused = lax.scan(absorb_one_step, running, (key_blocks, value_blocks))
    maxima, denoms, numerator = running
    ratio = numerator / denoms[..., None]
    diff = ratio[:, 0] - mix_lambda[:, None, None] * ratio[:, 1]
    normed = diff * lax.rsqrt(jnp.mean(diff * diff, axis=-1, keepdims=True) + EPSILON) * attn_gain
    attn_out = (
        jnp.transpose(normed, (1, 0, 2))
        .reshape(row_count, head_count * DA_VAL)
        .astype(jnp.bfloat16)
    )
    rec_q = jax.nn.silu(heads(query_rec, HG_KEY)) * HG_KEY ** (-0.5)
    values_rec = heads(value_rec, HG_VAL)
    zero_state = jnp.zeros((rec_heads, HG_KEY, HG_VAL), jnp.float32)
    identity = (jnp.zeros((rec_heads, HG_KEY), jnp.float32), zero_state)

    def prepare(forget, direction):
        gap = gate_gap[direction].reshape(rec_heads, HG_KEY)
        key_in = gap * jax.nn.sigmoid(-heads(forget, HG_KEY))
        log_decay = jnp.log1p(-key_in) + extra_decay[direction][:, :, None]
        return (key_in, log_decay)

    def finish(ordered_query, local_out, ordered_decay, incoming, start_state):
        entering_state = jnp.exp(incoming[0])[..., None] * start_state + incoming[1]
        cumulative_decay = jnp.cumsum(ordered_decay, axis=0)
        return local_out + jnp.einsum(
            "ibe,bef->ibf",
            ordered_query * jnp.exp(cumulative_decay),
            entering_state,
            precision=EXACT_PRECISION,
        )

    key_fwd, decay_fwd = prepare(forget_fwd, 0)
    local_fwd, ending_fwd = block_scan(rec_q, key_fwd, values_rec, decay_fwd, zero_state)
    incoming_fwd = prefix(
        (jnp.sum(decay_fwd, axis=0), ending_fwd), "sp", combine_states, identity, False
    )
    out_fwd = finish(rec_q, local_fwd, decay_fwd, incoming_fwd, init_state[0])
    key_bwd, decay_bwd = prepare(forget_bwd, 1)
    reversed_q = rec_q[::-1]
    reversed_decay = decay_bwd[::-1]
    local_bwd, ending_bwd = block_scan(
        reversed_q, key_bwd[::-1], values_rec[::-1], reversed_decay, zero_state
    )
    incoming_bwd = prefix(
        (jnp.sum(decay_bwd, axis=0), ending_bwd), "sp", combine_states, identity, True
    )
    out_bwd = finish(reversed_q, local_bwd, reversed_decay, incoming_bwd, init_state[1])[::-1]
    rec_sum = out_fwd + out_bwd
    rec_normed = (
        rec_sum
        * lax.rsqrt(jnp.mean(rec_sum * rec_sum, axis=-1, keepdims=True) + EPSILON)
        * rec_gain
    )
    rec_out = rec_normed.reshape(row_count, rec_heads * HG_VAL).astype(jnp.bfloat16)
    attn_rows, rec_rows = (
        lax.all_to_all(attn_out, "tp", split_axis=0, concat_axis=1, tiled=True),
        lax.all_to_all(rec_out, "tp", split_axis=0, concat_axis=1, tiled=True),
    )
    part = attn_rows
    mixed = jnp.dot(
        part, lax.all_gather(out_attn, "tp", axis=0, tiled=True), preferred_element_type=jnp.float32
    )
    part = rec_rows
    mixed = mixed + jnp.dot(
        part, lax.all_gather(out_rec, "tp", axis=0, tiled=True), preferred_element_type=jnp.float32
    )
    return mixed.astype(jnp.bfloat16)


def solution(mesh):
    placed = (
        P("sp", "tp"),
        P(),
        P(None, "tp"),
        P(None, "tp"),
        P(None, "tp"),
        P("tp"),
        P(),
        P(None, "tp"),
        P(None, "tp"),
        P(None, "tp"),
        P(None, "tp"),
        P(None, "tp"),
        P(None, "sp", "tp"),
        P(None, "tp", None, None),
        P(),
        P("tp", None),
        P("tp", None),
    )
    return jax.shard_map(
        local, mesh=mesh, in_specs=placed, out_specs=P(("sp", "tp"), None), check_vma=False
    )
```

profile of v0, /device:TPU:0, one launch (start us, length us, event | category | flops | bytes accessed | tf_op | source)
XLA Modules:
  0.0 277.9 jit_solution(16707672340335798208)
XLA Ops:
  7.3 8.9 %all_gather.35 = bf16[128,2048]{1,0:T(8,128)(2,1)S(1)} all-gather(bf16[128,512]{1,0:T(8,128)(2,1)} %param.25), channel_id=1, replica_groups=mesh['sp'=8,'tp'=4] {'tp'}, dimensions={1}, use_global_device_ids=true | all-gather | bytes 655360 | tf_op jit(solution)/shard_map/all_gather | solution.py:102
  16.4 1.6 fusion.53
  18.0 31.9 %all_gather.37 = bf16[1024,256]{1,0:T(8,128)(2,1)S(1)} all-gather(bf16[128,256]{1,0:T(8,128)(2,1)S(1)} %fusion.53), channel_id=1, replica_groups=mesh['sp'=8,'tp'=4] {'sp'}, dimensions={0}, use_global_device_ids=true | all-gather | bytes 589824 | tf_op jit(solution)/shard_map/all_gather | solution.py:126
  52.8 31.2 %all_gather.36 = bf16[1024,256]{1,0:T(8,128)(2,1)S(1)} all-gather(bf16[128,256]{1,0:T(8,128)(2,1)S(1)} %fusion.52), channel_id=1, replica_groups=mesh['sp'=8,'tp'=4] {'sp'}, dimensions={0}, use_global_device_ids=true | all-gather | bytes 589824 | tf_op jit(solution)/shard_map/all_gather | solution.py:125
  85.4 1.7 fusion.47
  88.1 3.3 %all-to-all-start = ((bf16[4,32,256]{2,1,0:T(8,128)(2,1)}), bf16[4,32,256]{2,1,0:T(8,128)(2,1)S(1)}, u32[]{:S(2)}, u32[]{:S(2)}) async-start(bf16[4,32,256]{2,1,0:T(8,128)(2,1)} %convert_element_type.144), calls=%async_computation | async-start | bytes 131072 | tf_op jit(solution)/shard_map/all_to_all | solution.py:205
  98.4 27.3 %while.60 = (s32[]{:T(128)}, f32[2,128,128]{2,1,0:T(8,128)S(1)}, f32[2,64,2,128]{3,1,0,2:T(8,128)S(1)}, f32[2,64,2,128]{3,2,1,0:T(2,128)S(1)}, f32[2,64,2,128]{3...) while((s32[]{:T(128)}, f32[2,128,128]{2,1,0:T(8,128)S(1)}, ...), condition=%wide.region_6.7_spmd.clone, body=%wide.region_4.6_spmd.clone.sunk | while | flops 79884288 | bytes 10336384 | solution.py:71
  99.3 5.9 %multiply_bitcast_fusion.4 = f32[64,2,128,64]{2,1,0,3:T(2,128)S(1)} fusion(pred[64,64]{1,0:T(8,128)(4,1)S(1)} %select_compare_fusion.4, f32[64,2,128]{2,1,0:T(2,128)S(1)} %get-tuple-element.582, f32[64,2,128]{2,1,0:T(2,128)S(1)} %fusion.159), kind=kLoop, calls=%fused_computation.12.clone.1 | loop fusion | flops 3145728 | bytes 4329472 | tf_op jit(solution)/shard_map/while/body/eval_jaxpr/ihk,ijhk,jhk->hij/dot_general | solution.py:53
  105.2 6.6 %fusion.161 = f32[2,64,1,64]{3,2,1,0:T(1,128)S(1)} fusion(f32[64,2,128,64]{2,1,0,3:T(2,128)S(1)} %multiply_bitcast_fusion.4, f32[64,2,128,1]{2,1,0,3:T(2,128)S(1)} %get-tuple-element.583), kind=kOutput, calls=%fused_computation.10.clone.1 | convolution fusion | flops 12582912 | bytes 4292608 | tf_op jit(solution)/shard_map/while/body/eval_jaxpr/ihk,ijhk,jhk->hij/dot_general | solution.py:53
  112.9 5.9 %multiply_bitcast_fusion.4 = f32[64,2,128,64]{2,1,0,3:T(2,128)S(1)} fusion(pred[64,64]{1,0:T(8,128)(4,1)S(1)} %select_compare_fusion.4, f32[64,2,128]{2,1,0:T(2,128)S(1)} %get-tuple-element.582, f32[64,2,128]{2,1,0:T(2,128)S(1)} %fusion.159), kind=kLoop, calls=%fused_computation.12.clone.1 | loop fusion | flops 3145728 | bytes 4329472 | tf_op jit(solution)/shard_map/while/body/eval_jaxpr/ihk,ijhk,jhk->hij/dot_general | solution.py:53
  118.9 6.6 %fusion.161 = f32[2,64,1,64]{3,2,1,0:T(1,128)S(1)} fusion(f32[64,2,128,64]{2,1,0,3:T(2,128)S(1)} %multiply_bitcast_fusion.4, f32[64,2,128,1]{2,1,0,3:T(2,128)S(1)} %get-tuple-element.583), kind=kOutput, calls=%fused_computation.10.clone.1 | convolution fusion | flops 12582912 | bytes 4292608 | tf_op jit(solution)/shard_map/while/body/eval_jaxpr/ihk,ijhk,jhk->hij/dot_general | solution.py:53
  125.9 27.6 %while.61 = (s32[]{:T(128)}, f32[2,128,128]{2,1,0:T(8,128)S(1)}, f32[2,64,2,128]{3,1,0,2:T(8,128)S(1)}, f32[2,64,2,128]{3,2,1,0:T(2,128)S(1)}, f32[2,64,2,128]{3...) while((s32[]{:T(128)}, f32[2,128,128]{2,1,0:T(8,128)S(1)}, ...), condition=%wide.region_13.14_spmd.clone, body=%wide.region_11.13_spmd.clone.sunk | while | flops 79884288 | bytes 10206336 | solution.py:71
  127.0 5.9 %multiply_bitcast_fusion.5 = f32[64,2,128,64]{2,1,0,3:T(2,128)S(1)} fusion(pred[64,64]{1,0:T(8,128)(4,1)S(1)} %select_compare_fusion.5, f32[64,2,128]{2,1,0:T(2,128)S(1)} %get-tuple-element.593, f32[64,2,128]{2,1,0:T(2,128)S(1)} %fusion.172), kind=kLoop, calls=%fused_computation.42.clone.1 | loop fusion | flops 3145728 | bytes 4329472 | tf_op jit(solution)/shard_map/while/body/eval_jaxpr/ihk,ijhk,jhk->hij/dot_general | solution.py:53
  132.9 6.6 %fusion.174 = f32[2,64,1,64]{3,2,1,0:T(1,128)S(1)} fusion(f32[64,2,128,64]{2,1,0,3:T(2,128)S(1)} %multiply_bitcast_fusion.5, f32[64,2,128,1]{2,1,0,3:T(2,128)S(1)} %dynamic-slice_bitcast_fusion.9), kind=kOutput, calls=%fused_computation.40.clone.1 | convolution fusion | flops 12582912 | bytes 4292608 | tf_op jit(solution)/shard_map/while/body/eval_jaxpr/ihk,ijhk,jhk->hij/dot_general | solution.py:53
  140.7 5.9 %multiply_bitcast_fusion.5 = f32[64,2,128,64]{2,1,0,3:T(2,128)S(1)} fusion(pred[64,64]{1,0:T(8,128)(4,1)S(1)} %select_compare_fusion.5, f32[64,2,128]{2,1,0:T(2,128)S(1)} %get-tuple-element.593, f32[64,2,128]{2,1,0:T(2,128)S(1)} %fusion.172), kind=kLoop, calls=%fused_computation.42.clone.1 | loop fusion | flops 3145728 | bytes 4329472 | tf_op jit(solution)/shard_map/while/body/eval_jaxpr/ihk,ijhk,jhk->hij/dot_general | solution.py:53
  146.6 6.6 %fusion.174 = f32[2,64,1,64]{3,2,1,0:T(1,128)S(1)} fusion(f32[64,2,128,64]{2,1,0,3:T(2,128)S(1)} %multiply_bitcast_fusion.5, f32[64,2,128,1]{2,1,0,3:T(2,128)S(1)} %dynamic-slice_bitcast_fusion.9), kind=kOutput, calls=%fused_computation.40.clone.1 | convolution fusion | flops 12582912 | bytes 4292608 | tf_op jit(solution)/shard_map/while/body/eval_jaxpr/ihk,ijhk,jhk->hij/dot_general | solution.py:53
  153.7 20.6 %all_gather.42 = bf16[8,2,128]{2,1,0:T(2,128)(2,1)S(1)} all-gather(bf16[1,2,128]{2,1,0:T(2,128)(2,1)S(1)} %bitcast.287), channel_id=1, replica_groups=mesh['sp'=8,'tp'=4] {'sp'}, dimensions={0}, use_global_device_ids=true | all-gather | bytes 4608 | tf_op jit(solution)/shard_map/all_gather | solution.py:21
  174.3 31.3 %all-gather.1 = bf16[16,128,128]{2,1,0:T(8,128)(2,1)S(1)} all-gather(bf16[2,128,128]{2,1,0:T(8,128)(2,1)S(1)} %convert_element_type.158), channel_id=3, replica_groups=mesh['sp'=8,'tp'=4] {'sp'}, dimensions={0}, use_global_device_ids=true | all-gather | bytes 589824 | tf_op jit(solution)/shard_map/all_gather | solution.py:21
  207.6 16.3 %all_gather.39 = bf16[8,2,128]{2,1,0:T(2,128)(2,1)S(1)} all-gather(bf16[1,2,128]{2,1,0:T(2,128)(2,1)S(1)} %bitcast.286), channel_id=1, replica_groups=mesh['sp'=8,'tp'=4] {'sp'}, dimensions={0}, use_global_device_ids=true | all-gather | bytes 4608 | tf_op jit(solution)/shard_map/all_gather | solution.py:21
  223.9 31.2 %all-gather = bf16[16,128,128]{2,1,0:T(8,128)(2,1)S(1)} all-gather(bf16[2,128,128]{2,1,0:T(8,128)(2,1)S(1)} %convert_element_type.153), channel_id=2, replica_groups=mesh['sp'=8,'tp'=4] {'sp'}, dimensions={0}, use_global_device_ids=true | all-gather | bytes 589824 | tf_op jit(solution)/shard_map/all_gather | solution.py:21
  256.8 3.4 %all-to-all-start.1 = ((bf16[4,32,256]{2,1,0:T(8,128)(2,1)}), bf16[4,32,256]{2,1,0:T(8,128)(2,1)S(1)}, u32[]{:S(2)}, u32[]{:S(2)}) async-start(bf16[4,32,256]{2,1,0:T(8,128)(2,1)} %convert_element_type.160), calls=%async_computation.1 | async-start | bytes 131072 | tf_op jit(solution)/shard_map/all_to_all | solution.py:206
  260.2 4.1 %all-to-all-done.1 = bf16[4,32,256]{2,1,0:T(8,128)(2,1)S(1)} async-done(((bf16[4,32,256]{2,1,0:T(8,128)(2,1)}), bf16[4,32,256]{2,1,0:T(8,128)(2,1)S(1)}, u32[]{:S(2)}, u32[]{:S(2)}) %all-to-all-start.1) | async-done | bytes 65568 | tf_op jit(solution)/shard_map/all_to_all | solution.py:206
  264.3 3.0 %fusion.109 = f32[32,2048]{1,0:T(8,128)S(1)} fusion(bf16[32,1024]{1,0:T(8,128)(2,1)S(1)} %bitcast.273, bf16[1024,2048]{1,0:T(8,128)(2,1)} %all-gather.5.cloned.1.call-done), kind=kOutput, calls=%fused_computation.170 | convolution fusion | flops 134217728 | bytes 4521984 | tf_op jit(solution)/shard_map/dot_general | solution.py:209
  267.4 3.7 %fusion.44 = bf16[32,2048]{1,0:T(8,128)(2,1)} fusion(f32[32,2048]{1,0:T(8,128)S(1)} %fusion.109, bf16[32,1024]{1,0:T(8,128)(2,1)S(1)} %bitcast.274, bf16[1024,2048]{1,0:T(8,128)(2,1)} %all-gather.7.cloned.1.call-done), kind=kOutput, calls=%fused_computation.75 | convolution fusion | flops 134348800 | bytes 4653056 | tf_op jit(solution)/shard_map/dot_general | solution.py:213
  (144 shorter events, 22.2 us)
Async XLA Ops:
  6.5 88.1 %copy-start = (bf16[2048,256]{1,0:T(8,128)(2,1)S(1)}, bf16[2048,256]{1,0:T(8,128)(2,1)}, u32[]{:S(2)}) copy-start(bf16[2048,256]{1,0:T(8,128)(2,1)} %param.34) | copy-start | bytes 3145732
  6.5 44.3 %copy-start.4 = (f32[2048]{0:T(1024)S(1)}, f32[2048]{0:T(1024)}, u32[]{:S(2)}) copy-start(f32[2048]{0:T(1024)} %param.26) | copy-start | bytes 24580
  6.5 44.3 %copy-start.1 = (bf16[2048,256]{1,0:T(8,128)(2,1)S(1)}, bf16[2048,256]{1,0:T(8,128)(2,1)}, u32[]{:S(2)}) copy-start(bf16[2048,256]{1,0:T(8,128)(2,1)} %param.27) | copy-start | bytes 3145732
  6.5 257.8 %all-gather.5.cloned.1.call-start = ((), (), s32[]{:S(2)}) async-start(), calls=%async_computation.2 | async-start | bytes 5242880 | tf_op jit(solution)/shard_map/all_gather | solution.py:210
  84.2 2.8 %copy-start.5 = (f32[2]{0:T(128)S(1)}, f32[2]{0:T(128)}, u32[]{:S(2)}) copy-start(f32[2]{0:T(128)} %param.30) | copy-start | bytes 28
  84.3 2.9 %copy-start.8 = (f32[128]{0:T(128)S(1)}, f32[128]{0:T(128)}, u32[]{:S(2)}) copy-start(f32[128]{0:T(128)} %param.31) | copy-start | bytes 1540
  84.8 7.3 %copy-start.2 = (bf16[2048,256]{1,0:T(8,128)(2,1)S(1)}, bf16[2048,256]{1,0:T(8,128)(2,1)}, u32[]{:S(2)}) copy-start(bf16[2048,256]{1,0:T(8,128)(2,1)} %param.32) | copy-start | bytes 3145732
  85.4 8.9 %copy-start.6 = (f32[2,128,2]{1,2,0:T(2,128)S(1)}, f32[2,128,2]{1,2,0:T(2,128)}, u32[]{:S(2)}) copy-start(f32[2,128,2]{1,2,0:T(2,128)} %param.37) | copy-start | bytes 6148
  85.4 9.1 %copy-start.7 = (f32[2,256]{1,0:T(2,128)S(1)}, f32[2,256]{1,0:T(2,128)}, u32[]{:S(2)}) copy-start(f32[2,256]{1,0:T(2,128)} %param.36) | copy-start | bytes 6148
  88.1 168.7 %all-to-all-start = ((bf16[4,32,256]{2,1,0:T(8,128)(2,1)}), bf16[4,32,256]{2,1,0:T(8,128)(2,1)S(1)}, u32[]{:S(2)}, u32[]{:S(2)}) async-start(bf16[4,32,256]{2,1,0:T(8,128)(2,1)} %convert_element_type.144), calls=%async_computation | async-start | bytes 131072 | tf_op jit(solution)/shard_map/all_to_all | solution.py:205
  91.4 176.0 %all-gather.7.cloned.1.call-start = ((), (), s32[]{:S(2)}) async-start(), calls=%async_computation.3 | async-start | bytes 5242880 | tf_op jit(solution)/shard_map/all_gather | solution.py:214
  125.9 81.0 %copy-start.3 = (f32[2,2,128,128]{3,2,1,0:T(8,128)S(1)}, f32[2,2,128,128]{3,2,1,0:T(8,128)}, u32[]{:S(2)}) copy-start(f32[2,2,128,128]{3,2,1,0:T(8,128)} %param.38) | copy-start | bytes 786436
  153.5 102.4 %copy-start.9 = (f32[128]{0:T(128)S(1)}, f32[128]{0:T(128)}, u32[]{:S(2)}) copy-start(f32[128]{0:T(128)} %param.39) | copy-start | bytes 1540
  256.8 7.5 %all-to-all-start.1 = ((bf16[4,32,256]{2,1,0:T(8,128)(2,1)}), bf16[4,32,256]{2,1,0:T(8,128)(2,1)S(1)}, u32[]{:S(2)}, u32[]{:S(2)}) async-start(bf16[4,32,256]{2,1,0:T(8,128)(2,1)} %convert_element_type.160), calls=%async_computation.1 | async-start | bytes 131072 | tf_op jit(solution)/shard_map/all_to_all | solution.py:206
Sparse Core Ops, SparseCore 0:
  8.9 37.1 all-gather.4
  93.8 36.0 all-gather.6
where the time goes:
time: 278 us
  blocking collectives  171 us (62%)
  matrix products  47 us (17%)
  other arithmetic  27.7 us (10%)
  between operations  13.9 us (5%)
  starting transfers between devices  6.87 us (2%)
  waiting for transfers between devices  5.34 us (2%)
  local copies, waits for them, and re-layouts  4.9 us (2%)
    all_gather x4, blocking collectives, prefix(): lax.all_gather(a.astype(kind), axis)  99.4 us
    all_gather x1, blocking collectives, local(): value_piece = lax.all_gather(value_att, 'sp', axis=0, tiled=True)  31.9 us
    all_gather x1, blocking collectives, local(): key_piece = lax.all_gather(key_att, 'sp', axis=0, tiled=True)  31.2 us
    dot_general x4, matrix products, block_one_step(): jnp.einsum('ihk,ijhk,jhk->hij', query_tile, jnp.exp(relative), key_tile,...  26.5 us
    dot_general x4, other arithmetic, block_one_step(): jnp.einsum('ihk,ijhk,jhk->hij', query_tile, jnp.exp(relative), key_tile,...  23.6 us
    all_gather x1, blocking collectives, local(): lax.all_gather(tokens, 'tp', axis=1, tiled=True).astype(jnp.float32)  8.89 us
    dot_general x7, matrix products, local(): jnp.dot(scaled, weight, preferred_element_type=jnp.float32)  7.32 us
  transfers between devices with their start and end apart: 4, of which 1 were waited for; matrix products, arithmetic and copies ran while one was open for 27% of the time, Pallas kernels for 0%

commit v1 on v0

--- a/solution.py
+++ b/solution.py
@@ -122,8 +122,11 @@
         jnp.zeros((head_count, 2, row_count, DA_VAL), jnp.float32),
     )
     running = start_state
-    key_piece = lax.all_gather(key_att, "sp", axis=0, tiled=True)
-    value_piece = lax.all_gather(value_att, "sp", axis=0, tiled=True)
+    key_piece, value_piece = jnp.split(
+        lax.all_gather(jnp.concatenate([key_att, value_att], axis=1), "sp", axis=0, tiled=True),
+        [key_att.shape[1]],
+        axis=1,
+    )
     length = key_piece.shape[0]
     step_rows = max((candidate for candidate in range(1, 2049) if length % candidate == 0))
     key_blocks = key_piece.reshape(length // step_rows, step_rows, head_count, 2, QK_DIM)

time: 278 us -> 232 us (0.83)
  blocking collectives: 171 us -> 110 us
  other arithmetic: 27.7 us -> 35.1 us
  local copies, waits for them, and re-layouts: 4.9 us -> 11.2 us
    all_gather x2 -> x0, blocking collectives: 63.1 us -> none  [the longest x1 31.9 us: local(): value_piece = lax.all_gather(value_att, 'sp', axis=0, tiled=True)]
    exp x7, other arithmetic: 0.12 us -> 4.61 us  [combine_states(): jnp.exp(later[0])[..., None] * earlier[1] + later[1]]
    all_to_all x1, waiting for transfers between devices: 4.11 us -> 0.01 us  [local(): lax.all_to_all(rec_out, 'tp', split_axis=0, concat_axis=1, tiled=True)]
    all_to_all x1, waiting for transfers between devices: 0.01 us -> 4.07 us  [local(): lax.all_to_all(attn_out, 'tp', split_axis=0, concat_axis=1, tiled=True)]
  transfers between devices with their start and end apart: 4 -> 5, of which waited for: 1 -> 1; matrix products, arithmetic and copies ran while one was open for 27% -> 37% of each run, Pallas kernels for 0% -> 0%
where the time goes in v1:
time: 232 us; the launch traced here: 231 us
  blocking collectives  110 us (47%)
  matrix products  48.6 us (21%)
  other arithmetic  35.1 us (15%)
  between operations  13.6 us (6%)
  local copies, waits for them, and re-layouts  11.2 us (5%)
  starting transfers between devices  6.65 us (3%)
  waiting for transfers between devices  5.49 us (2%)
    all_gather x4, blocking collectives, prefix(): lax.all_gather(a.astype(kind), axis)  101 us
    dot_general x4, matrix products, block_one_step(): jnp.einsum('ihk,ijhk,jhk->hij', query_tile, jnp.exp(relative), key_tile,...  26.5 us
    dot_general x4, other arithmetic, block_one_step(): jnp.einsum('ihk,ijhk,jhk->hij', query_tile, jnp.exp(relative), key_tile,...  23.6 us
    all_gather x1, blocking collectives, local(): lax.all_gather(tokens, 'tp', axis=1, tiled=True).astype(jnp.float32)  9.02 us
    dot_general x7, matrix products, local(): jnp.dot(scaled, weight, preferred_element_type=jnp.float32)  7.89 us
  transfers between devices with their start and end apart: 5, of which 1 were waited for; matrix products, arithmetic and copies ran while one was open for 37% of the time, Pallas kernels for 0%

profile of v1, /device:TPU:0, one launch (start us, length us, event | category | flops | bytes accessed | tf_op | source)
XLA Modules:
  0.0 231.0 jit_solution(14156314115511426537)
XLA Ops:
  6.5 9.0 %all_gather.32 = bf16[128,2048]{1,0:T(8,128)(2,1)S(1)} all-gather(bf16[128,512]{1,0:T(8,128)(2,1)} %param.25), channel_id=1, replica_groups=mesh['sp'=8,'tp'=4] {'tp'}, dimensions={1}, use_global_device_ids=true | all-gather | bytes 655360 | tf_op jit(solution)/shard_map/all_gather | solution.py:102
  25.6 27.3 %while.61 = (s32[]{:T(128)}, f32[2,128,128]{2,1,0:T(8,128)S(1)}, f32[2,64,2,128]{3,1,0,2:T(8,128)S(1)}, f32[2,64,2,128]{3,2,1,0:T(2,128)S(1)}, f32[2,64,2,128]{3...) while((s32[]{:T(128)}, f32[2,128,128]{2,1,0:T(8,128)S(1)}, ...), condition=%wide.region_13.14_spmd.clone, body=%wide.region_11.13_spmd.clone.sunk | while | flops 79884288 | bytes 10206336 | solution.py:71
  26.5 5.9 %multiply_bitcast_fusion.5 = f32[64,2,128,64]{2,1,0,3:T(2,128)S(1)} fusion(pred[64,64]{1,0:T(8,128)(4,1)S(1)} %select_compare_fusion.5, f32[64,2,128]{2,1,0:T(2,128)S(1)} %get-tuple-element.595, f32[64,2,128]{2,1,0:T(2,128)S(1)} %fusion.173), kind=kLoop, calls=%fused_computation.42.clone.1 | loop fusion | flops 3145728 | bytes 4329472 | tf_op jit(solution)/shard_map/while/body/eval_jaxpr/ihk,ijhk,jhk->hij/dot_general | solution.py:53
  32.4 6.6 %fusion.175 = f32[2,64,1,64]{3,2,1,0:T(1,128)S(1)} fusion(f32[64,2,128,64]{2,1,0,3:T(2,128)S(1)} %multiply_bitcast_fusion.5, f32[64,2,128,1]{2,1,0,3:T(2,128)S(1)} %dynamic-slice_bitcast_fusion.9), kind=kOutput, calls=%fused_computation.40.clone.1 | convolution fusion | flops 12582912 | bytes 4292608 | tf_op jit(solution)/shard_map/while/body/eval_jaxpr/ihk,ijhk,jhk->hij/dot_general | solution.py:53
  40.2 5.9 %multiply_bitcast_fusion.5 = f32[64,2,128,64]{2,1,0,3:T(2,128)S(1)} fusion(pred[64,64]{1,0:T(8,128)(4,1)S(1)} %select_compare_fusion.5, f32[64,2,128]{2,1,0:T(2,128)S(1)} %get-tuple-element.595, f32[64,2,128]{2,1,0:T(2,128)S(1)} %fusion.173), kind=kLoop, calls=%fused_computation.42.clone.1 | loop fusion | flops 3145728 | bytes 4329472 | tf_op jit(solution)/shard_map/while/body/eval_jaxpr/ihk,ijhk,jhk->hij/dot_general | solution.py:53
  46.1 6.6 %fusion.175 = f32[2,64,1,64]{3,2,1,0:T(1,128)S(1)} fusion(f32[64,2,128,64]{2,1,0,3:T(2,128)S(1)} %multiply_bitcast_fusion.5, f32[64,2,128,1]{2,1,0,3:T(2,128)S(1)} %dynamic-slice_bitcast_fusion.9), kind=kOutput, calls=%fused_computation.40.clone.1 | convolution fusion | flops 12582912 | bytes 4292608 | tf_op jit(solution)/shard_map/while/body/eval_jaxpr/ihk,ijhk,jhk->hij/dot_general | solution.py:53
  53.0 21.2 %all_gather.38 = bf16[8,2,128]{2,1,0:T(2,128)(2,1)} all-gather(bf16[1,2,128]{2,1,0:T(2,128)(2,1)S(1)} %bitcast.287), channel_id=1, replica_groups=mesh['sp'=8,'tp'=4] {'sp'}, dimensions={0}, use_global_device_ids=true | all-gather | bytes 4608 | tf_op jit(solution)/shard_map/all_gather | solution.py:21
  74.2 31.8 %all-gather.1 = bf16[16,128,128]{2,1,0:T(8,128)(2,1)S(1)} all-gather(bf16[2,128,128]{2,1,0:T(8,128)(2,1)S(1)} %convert_element_type.158), channel_id=3, replica_groups=mesh['sp'=8,'tp'=4] {'sp'}, dimensions={0}, use_global_device_ids=true | all-gather | bytes 589824 | tf_op jit(solution)/shard_map/all_gather | solution.py:21
  106.4 2.2 fusion.74
  109.7 27.3 %while.60 = (s32[]{:T(128)}, f32[2,128,128]{2,1,0:T(8,128)S(1)}, f32[2,64,2,128]{3,1,0,2:T(8,128)S(1)}, f32[2,64,2,128]{3,2,1,0:T(2,128)S(1)}, f32[2,64,2,128]{3...) while((s32[]{:T(128)}, f32[2,128,128]{2,1,0:T(8,128)S(1)}, ...), condition=%wide.region_6.7_spmd.clone, body=%wide.region_4.6_spmd.clone.sunk | while | flops 79884288 | bytes 10336384 | solution.py:71
  110.6 5.9 %multiply_bitcast_fusion.4 = f32[64,2,128,64]{2,1,0,3:T(2,128)S(1)} fusion(pred[64,64]{1,0:T(8,128)(4,1)S(1)} %select_compare_fusion.4, f32[64,2,128]{2,1,0:T(2,128)S(1)} %get-tuple-element.584, f32[64,2,128]{2,1,0:T(2,128)S(1)} %fusion.160), kind=kLoop, calls=%fused_computation.12.clone.1 | loop fusion | flops 3145728 | bytes 4329472 | tf_op jit(solution)/shard_map/while/body/eval_jaxpr/ihk,ijhk,jhk->hij/dot_general | solution.py:53
  116.5 6.6 %fusion.162 = f32[2,64,1,64]{3,2,1,0:T(1,128)S(1)} fusion(f32[64,2,128,64]{2,1,0,3:T(2,128)S(1)} %multiply_bitcast_fusion.4, f32[64,2,128,1]{2,1,0,3:T(2,128)S(1)} %get-tuple-element.585), kind=kOutput, calls=%fused_computation.10.clone.1 | convolution fusion | flops 12582912 | bytes 4292608 | tf_op jit(solution)/shard_map/while/body/eval_jaxpr/ihk,ijhk,jhk->hij/dot_general | solution.py:53
  124.3 5.9 %multiply_bitcast_fusion.4 = f32[64,2,128,64]{2,1,0,3:T(2,128)S(1)} fusion(pred[64,64]{1,0:T(8,128)(4,1)S(1)} %select_compare_fusion.4, f32[64,2,128]{2,1,0:T(2,128)S(1)} %get-tuple-element.584, f32[64,2,128]{2,1,0:T(2,128)S(1)} %fusion.160), kind=kLoop, calls=%fused_computation.12.clone.1 | loop fusion | flops 3145728 | bytes 4329472 | tf_op jit(solution)/shard_map/while/body/eval_jaxpr/ihk,ijhk,jhk->hij/dot_general | solution.py:53
  130.2 6.6 %fusion.162 = f32[2,64,1,64]{3,2,1,0:T(1,128)S(1)} fusion(f32[64,2,128,64]{2,1,0,3:T(2,128)S(1)} %multiply_bitcast_fusion.4, f32[64,2,128,1]{2,1,0,3:T(2,128)S(1)} %get-tuple-element.585), kind=kOutput, calls=%fused_computation.10.clone.1 | convolution fusion | flops 12582912 | bytes 4292608 | tf_op jit(solution)/shard_map/while/body/eval_jaxpr/ihk,ijhk,jhk->hij/dot_general | solution.py:53
  137.7 5.7 %while.59 = (s32[]{:T(128)}, f32[2,128]{1,0:T(2,128)S(1)}, f32[2,128,128]{2,1,0:T(8,128)S(1)}, s32[]{:T(128)}, bf16[8,2,128]{2,1,0:T(2,128)(2,1)}, /*index=5*/bf...) while((s32[]{:T(128)}, f32[2,128]{1,0:T(2,128)S(1)}, ...), condition=%wide.region_16.17_spmd, body=%wide.region_15.16_spmd.sunk | while | flops 98822 | bytes 332451 | solution.py:36
  143.4 1.6 div.62
  148.3 1.7 copy.78
  150.0 16.6 %all_gather.35 = bf16[8,2,128]{2,1,0:T(2,128)(2,1)S(1)} all-gather(bf16[1,2,128]{2,1,0:T(2,128)(2,1)} %bitcast.286), channel_id=1, replica_groups=mesh['sp'=8,'tp'=4] {'sp'}, dimensions={0}, use_global_device_ids=true | all-gather | bytes 4608 | tf_op jit(solution)/shard_map/all_gather | solution.py:21
  166.6 31.2 %all-gather = bf16[16,128,128]{2,1,0:T(8,128)(2,1)S(1)} all-gather(bf16[2,128,128]{2,1,0:T(8,128)(2,1)S(1)} %convert_element_type.153), channel_id=2, replica_groups=mesh['sp'=8,'tp'=4] {'sp'}, dimensions={0}, use_global_device_ids=true | all-gather | bytes 589824 | tf_op jit(solution)/shard_map/all_gather | solution.py:21
  202.1 3.3 %all-to-all-start.1 = ((bf16[4,32,256]{2,1,0:T(8,128)(2,1)}), bf16[4,32,256]{2,1,0:T(8,128)(2,1)S(1)}, u32[]{:S(2)}, u32[]{:S(2)}) async-start(bf16[4,32,256]{2,1,0:T(8,128)(2,1)} %convert_element_type.160), calls=%async_computation.1 | async-start | bytes 131072 | tf_op jit(solution)/shard_map/all_to_all | solution.py:209
  210.4 3.3 %all-to-all-start = ((bf16[4,32,256]{2,1,0:T(8,128)(2,1)}), bf16[4,32,256]{2,1,0:T(8,128)(2,1)S(1)}, u32[]{:S(2)}, u32[]{:S(2)}) async-start(bf16[4,32,256]{2,1,0:T(8,128)(2,1)} %convert_element_type.144), calls=%async_computation | async-start | bytes 131072 | tf_op jit(solution)/shard_map/all_to_all | solution.py:208
  213.7 4.1 %all-to-all-done = bf16[4,32,256]{2,1,0:T(8,128)(2,1)S(1)} async-done(((bf16[4,32,256]{2,1,0:T(8,128)(2,1)}), bf16[4,32,256]{2,1,0:T(8,128)(2,1)S(1)}, u32[]{:S(2)}, u32[]{:S(2)}) %all-to-all-start) | async-done | bytes 65568 | tf_op jit(solution)/shard_map/all_to_all | solution.py:208
  217.8 3.0 %fusion.110 = f32[32,2048]{1,0:T(8,128)S(1)} fusion(bf16[32,1024]{1,0:T(8,128)(2,1)S(1)} %bitcast.274, bf16[1024,2048]{1,0:T(8,128)(2,1)} %all-gather.8.cloned.1.call-done), kind=kOutput, calls=%fused_computation.172 | convolution fusion | flops 134217728 | bytes 4521984 | tf_op jit(solution)/shard_map/dot_general | solution.py:212
  220.8 3.7 %fusion.44 = bf16[32,2048]{1,0:T(8,128)(2,1)} fusion(f32[32,2048]{1,0:T(8,128)S(1)} %fusion.110, bf16[32,1024]{1,0:T(8,128)(2,1)S(1)} %bitcast.273, bf16[1024,2048]{1,0:T(8,128)(2,1)} %all-gather.10.cloned.1.call-done), kind=kOutput, calls=%fused_computation.75 | convolution fusion | flops 134348800 | bytes 4653056 | tf_op jit(solution)/shard_map/dot_general | solution.py:216
  (155 shorter events, 34.1 us)
Async XLA Ops:
  6.5 17.1 %copy-start = (bf16[2048,256]{1,0:T(8,128)(2,1)S(1)}, bf16[2048,256]{1,0:T(8,128)(2,1)}, u32[]{:S(2)}) copy-start(bf16[2048,256]{1,0:T(8,128)(2,1)} %param.34) | copy-start | bytes 3145732
  6.5 14.6 %copy-start.8 = (f32[2048]{0:T(1024)S(1)}, f32[2048]{0:T(1024)}, u32[]{:S(2)}) copy-start(f32[2048]{0:T(1024)} %param.26) | copy-start | bytes 24580
  6.5 14.6 %copy-start.1 = (bf16[2048,256]{1,0:T(8,128)(2,1)S(1)}, bf16[2048,256]{1,0:T(8,128)(2,1)}, u32[]{:S(2)}) copy-start(bf16[2048,256]{1,0:T(8,128)(2,1)} %param.32) | copy-start | bytes 3145732
  6.5 199.3 %all-gather.6.cloned.1.call-start = ((), (), s32[]{:S(2)}) async-start(), calls=%async_computation.2 | async-start | bytes 1179648 | tf_op jit(solution)/shard_map/all_gather | solution.py:126
  17.3 5.9 %copy-start.11 = (f32[2,128,2]{1,2,0:T(2,128)S(1)}, f32[2,128,2]{1,2,0:T(2,128)}, u32[]{:S(2)}) copy-start(f32[2,128,2]{1,2,0:T(2,128)} %param.37) | copy-start | bytes 6148
  17.3 6.0 %copy-start.12 = (f32[2,256]{1,0:T(2,128)S(1)}, f32[2,256]{1,0:T(2,128)}, u32[]{:S(2)}) copy-start(f32[2,256]{1,0:T(2,128)} %param.36) | copy-start | bytes 6148
  19.6 198.1 %all-gather.8.cloned.1.call-start = ((), (), s32[]{:S(2)}) async-start(), calls=%async_computation.3 | async-start | bytes 5242880 | tf_op jit(solution)/shard_map/all_gather | solution.py:213
  20.4 200.4 %all-gather.10.cloned.1.call-start = ((), (), s32[]{:S(2)}) async-start(), calls=%async_computation.4 | async-start | bytes 5242880 | tf_op jit(solution)/shard_map/all_gather | solution.py:217
  23.4 85.9 %copy-start.9 = (f32[1,256]{1,0:T(1,128)}, f32[1,256]{1,0:T(1,128)S(1)}, u32[]{:S(2)}) copy-start(f32[1,256]{1,0:T(1,128)S(1)} %get-tuple-element.397) | copy-start | bytes 3076
  53.0 56.7 %copy-start.6 = (f32[2,64,2,128]{3,1,0,2:T(8,128)}, f32[2,64,2,128]{3,1,0,2:T(8,128)S(1)}, u32[]{:S(2)}) copy-start(f32[2,64,2,128]{3,1,0,2:T(8,128)S(1)} %get-tuple-element.231) | copy-start | bytes 393220
  106.2 2.5 %copy-start.3 = (f32[128,2]{1,0:T(8,128)}, f32[128,2]{1,0:T(8,128)S(1)}, u32[]{:S(2)}) copy-start(f32[128,2]{1,0:T(8,128)S(1)} %copy.75) | copy-start | bytes 3076
  108.6 0.7 copy-start.5
  137.0 0.6 copy-start.7
  137.7 67.7 %copy-start.2 = (bf16[2048,256]{1,0:T(8,128)(2,1)S(1)}, bf16[2048,256]{1,0:T(8,128)(2,1)}, u32[]{:S(2)}) copy-start(bf16[2048,256]{1,0:T(8,128)(2,1)} %param.27) | copy-start | bytes 3145732
  143.4 54.4 %copy-start.4 = (f32[128,2]{1,0:T(8,128)S(1)}, f32[128,2]{1,0:T(8,128)}, u32[]{:S(2)}) copy-start(f32[128,2]{1,0:T(8,128)} %copy-done.3) | copy-start | bytes 3076
  202.1 8.3 %all-to-all-start.1 = ((bf16[4,32,256]{2,1,0:T(8,128)(2,1)}), bf16[4,32,256]{2,1,0:T(8,128)(2,1)S(1)}, u32[]{:S(2)}, u32[]{:S(2)}) async-start(bf16[4,32,256]{2,1,0:T(8,128)(2,1)} %convert_element_type.160), calls=%async_computation.1 | async-start | bytes 131072 | tf_op jit(solution)/shard_map/all_to_all | solution.py:209
  207.6 1.7 copy-start.10
  207.6 1.9 copy-start.13
  210.4 7.4 %all-to-all-start = ((bf16[4,32,256]{2,1,0:T(8,128)(2,1)}), bf16[4,32,256]{2,1,0:T(8,128)(2,1)S(1)}, u32[]{:S(2)}, u32[]{:S(2)}) async-start(bf16[4,32,256]{2,1,0:T(8,128)(2,1)} %convert_element_type.144), calls=%async_computation | async-start | bytes 131072 | tf_op jit(solution)/shard_map/all_to_all | solution.py:208
Sparse Core Ops, SparseCore 0:
  19.7 41.1 all-gather.5
  62.4 33.1 all-gather.7
  97.2 34.4 all-gather.9
